TPU v7x, 256 devices: a whole 4x4x8 slice. The times are simulated.
256 devices in a mesh: ep: 64 (over z, y, core), tp: 4 (over x).
Axes of the slice: x: 4, y: 4, z: 8, core: 2. Of those that a mesh axis runs over, the one named last changes fastest.
Arguments:
- queries: bfloat16 [65536, 1024], P('ep', 'tp'), may hold values from -6 to 6
- head_keys: bfloat16 [65536, 256], P('ep', 'tp'), may hold values from -6 to 6
- head_values: bfloat16 [65536, 256], P('ep', 'tp'), may hold values from -6 to 6
- sink_logits: float32 [16], P('tp'), may hold values from -2 to 5
- out_weight: bfloat16 [1024, 2048], P('tp'), may hold values from -1.5 to 1.5
- moe_input: bfloat16 [32768, 2048], P(('ep', 'tp')), may hold values from -6 to 6
- norm_gain: float32 [2048], replicated, may hold values from 0.1 to 1.9
- routes: int32 [32768, 4], P(('ep', 'tp')), may hold values from 0 to 63, all different within a row; in each aligned block of 128 rows (0 to 127, 128 to 255, ...) at most 16 rows name the same one
- route_weight: float32 [32768, 4], P(('ep', 'tp')), may hold values from 0.05 to 1
- gate_weight: bfloat16 [64, 2048, 512], P('ep'), may hold values from -2 to 2
- up_weight: bfloat16 [64, 2048, 512], P('ep'), may hold values from -2 to 2
- down_weight: bfloat16 [64, 512, 2048], P('ep'), may hold values from -0.25 to 0.25
Outputs:
- attention_out: bfloat16 [65536, 2048], P(('ep', 'tp'))
- routed_out: bfloat16 [32768, 2048], P(('ep', 'tp'))
Inputs may be any that keep to these rules, and one draw needn't show every extreme that they name: `routes`: within the rows of one device (aligned blocks of 128 rows), each expert is named by at most 16 rows, and in every draw some expert by exactly 16; a row names 4 different experts.
All inputs are finite; a program needn't handle non-finite values.
Results may differ from a plain program's by a relative error of at most 0.0078.
Values may be sent and summed in bfloat16 or wider, within the bound.
A program may use at most 128 MiB of HBM per device.

v0:
```python
import jax
import jax.numpy as jnp
from jax import lax
from jax.sharding import PartitionSpec as P

HEAD_DIM = 64
WINDOW = 128
SEQS = 1


EPSILON = 1e-05
NEGATIVE = -1e30


def passed_along(value, axis, steps):
    count = lax.axis_size(axis)
    first, last = (max(0, -steps), min(count, count - steps))
    return lax.ppermute(value, axis, [(source, source + steps) for source in range(first, last)])


def clamped_unit(gate_pre, up_pre):
    gate_cut = jnp.minimum(gate_pre, 7.0)
    up_cut = jnp.clip(up_pre, -7.0, 7.0)
    return gate_cut * jax.nn.sigmoid(1.702 * gate_cut) * (up_cut + 1.0)


def attend(queries, head_keys, head_values, sink_logits, out_weight):
    tok_rows = queries.shape[0]
    local_heads = sink_logits.shape[0]
    local_kv = head_keys.shape[1] // HEAD_DIM
    per_group = local_heads // local_kv
    block_count = tok_rows // WINDOW
    key_width = local_kv * HEAD_DIM
    kv_rows = jnp.concatenate([head_keys, head_values], axis=1)
    earlier = passed_along(kv_rows[tok_rows - WINDOW :], "ep", 1)
    extended = jnp.concatenate([earlier, kv_rows], axis=0)
    banded = jnp.concatenate(
        [
            extended[:tok_rows].reshape(block_count, WINDOW, 2 * key_width),
            kv_rows.reshape(block_count, WINDOW, 2 * key_width),
        ],
        axis=1,
    )
    band_keys = banded[:, :, :key_width].reshape(block_count, 2 * WINDOW, local_kv, HEAD_DIM)
    band_values = banded[:, :, key_width:].reshape(block_count, 2 * WINDOW, local_kv, HEAD_DIM)
    blocked = queries.reshape(block_count, WINDOW, local_kv, per_group, HEAD_DIM)
    scores = jnp.einsum(
        "nqkgd,nskd->nkgqs", blocked, band_keys, preferred_element_type=jnp.float32
    ) * HEAD_DIM ** (-0.5)
    offset = lax.axis_index("ep") * tok_rows
    seq_len = tok_rows * lax.axis_size("ep") // SEQS
    query_pos = offset + jnp.arange(tok_rows, dtype=jnp.int32).reshape(block_count, WINDOW)
    key_pos = (
        offset
        - WINDOW
        + (jnp.arange(block_count, dtype=jnp.int32) * WINDOW)[:, None]
        + jnp.arange(2 * WINDOW, dtype=jnp.int32)[None, :]
    )
    distance = query_pos[:, :, None] - key_pos[:, None, :]
    starts = query_pos // seq_len * seq_len
    valid = (distance >= 0) & (distance < WINDOW) & (key_pos[:, None, :] >= starts[:, :, None])
    scores = jnp.where(valid[:, None, None], scores, NEGATIVE)
    sinks = sink_logits.reshape(local_kv, per_group, 1, 1)
    maxima = jnp.maximum(jnp.max(scores, axis=-1, keepdims=True), sinks)
    powers = jnp.exp(scores - maxima)
    weights = (powers / (jnp.sum(powers, axis=-1, keepdims=True) + jnp.exp(sinks - maxima))).astype(
        jnp.bfloat16
    )
    heads_out = jnp.einsum(
        "nkgqs,nskd->nqkgd", weights, band_values, preferred_element_type=jnp.float32
    )
    heads_out = heads_out.astype(jnp.bfloat16).reshape(tok_rows, local_heads * HEAD_DIM)
    summed = lax.psum_scatter(
        jnp.dot(heads_out, out_weight, preferred_element_type=jnp.float32),
        "tp",
        scatter_dimension=0,
        tiled=True,
    )
    return summed.astype(jnp.bfloat16)


def experts_part(moe_input, norm_gain, routes, route_weight, gate_weight, up_weight, down_weight):
    tok_rows, model_width = moe_input.shape
    choice_count = routes.shape[1]
    targets = lax.axis_size("ep")
    capacity = 2 * choice_count * tok_rows // targets
    values32 = moe_input.astype(jnp.float32)
    scale = lax.rsqrt(jnp.mean(values32 * values32, axis=-1, keepdims=True) + EPSILON)
    normed = (values32 * scale * norm_gain).astype(jnp.bfloat16)
    flat_routes = routes.reshape(-1)
    onehot = (flat_routes[:, None] == jnp.arange(targets, dtype=jnp.int32)[None, :]).astype(
        jnp.int32
    )
    earlier_count = jnp.sum((jnp.cumsum(onehot, axis=0) - onehot) * onehot, axis=1)
    slot_index = flat_routes * capacity + earlier_count
    copies = jnp.repeat(normed, choice_count, axis=0)
    outgoing = jnp.zeros((targets * capacity, model_width), jnp.bfloat16).at[slot_index].set(copies)
    outgoing = outgoing.reshape(targets, capacity, model_width)
    arrived = lax.all_to_all(outgoing, "ep", split_axis=0, concat_axis=0, tiled=True)
    flat_rows = arrived.reshape(-1, model_width)
    gate_pre = jnp.dot(flat_rows, gate_weight[0], preferred_element_type=jnp.float32)
    up_pre = jnp.dot(flat_rows, up_weight[0], preferred_element_type=jnp.float32)
    act = clamped_unit(gate_pre, up_pre).astype(jnp.bfloat16)
    result = jnp.dot(act, down_weight[0], preferred_element_type=jnp.float32).astype(jnp.bfloat16)
    came_back = lax.all_to_all(
        result.reshape(arrived.shape), "ep", split_axis=0, concat_axis=0, tiled=True
    )
    picked = came_back.reshape(targets * capacity, model_width)[slot_index]
    weighted = (
        picked.astype(jnp.float32).reshape(tok_rows, choice_count, model_width)
        * route_weight[:, :, None]
    )
    return jnp.sum(weighted, axis=1).astype(jnp.bfloat16)


def on_device(
    queries,
    head_keys,
    head_values,
    sink_logits,
    out_weight,
    moe_input,
    norm_gain,
    routes,
    route_weight,
    gate_weight,
    up_weight,
    down_weight,
):
    attention_out = attend(queries, head_keys, head_values, sink_logits, out_weight)
    routed_out = experts_part(
        moe_input, norm_gain, routes, route_weight, gate_weight, up_weight, down_weight
    )
    return (attention_out, routed_out)


def solution(mesh):
    placed = (
        P("ep", "tp"),
        P("ep", "tp"),
        P("ep", "tp"),
        P("tp"),
        P("tp", None),
        P(("ep", "tp"), None),
        P(),
        P(("ep", "tp"), None),
        P(("ep", "tp"), None),
        P("ep", None, None),
        P("ep", None, None),
        P("ep", None, None),
    )
    return jax.shard_map(
        on_device,
        mesh=mesh,
        in_specs=placed,
        out_specs=(P(("ep", "tp"), None), P(("ep", "tp"), None)),
        check_vma=False,
    )
```

profile of v0, /device:TPU:1, one launch (start us, length us, event | category | flops | bytes accessed | tf_op | source)
XLA Modules:
  0.0 288.0 jit_solution(10558214354519502273)
XLA Ops:
  7.2 1.2 copy.17
  8.4 1.2 copy.18
  9.7 4.6 %collective-permute-start = (bf16[128,128]{1,0:T(8,128)(2,1)S(1)}, bf16[128,128]{1,0:T(8,128)(2,1)S(1)}, u32[]{:S(2)}, u32[]{:S(2)}) collective-permute-start(bf16[128,128]{1,0:T(8,128)(2,1)S(1)} %fusion.42), channel_id=1, source_target_pairs={{0,4},{4,8},{8,12},{12,16},{16,20},{20,24},{24,28},{28,32},{32,36}... | collective-permute-start | bytes 98312 | tf_op jit(solution)/shard_map/ppermute | solution.py:18
  14.3 0.8 copy.26
  15.3 0.7 broadcast_multiply_fusion
  16.0 1.2 reduce-window.6
  17.2 0.2 slice_reduce_fusion
  17.7 1.2 fusion.20
  18.9 1.2 fusion.22
  20.2 2.4 broadcast_in_dim.19
  22.5 4.0 %reshape.229 = bf16[512,2048]{1,0:T(8,128)(2,1)} reshape(bf16[128,4,2048]{2,1,0:T(4,128)(2,1)} %broadcast_in_dim.19) | data formatting | bytes 4194304 | tf_op jit(solution)/shard_map/reshape | solution.py:96
  26.6 7.2 %scatter_custom_fusion = bf16[1024,2048]{1,0:T(8,128)(2,1)} fusion(s32[512]{0:T(512)S(1)} %bitcast.96, bf16[512,2048]{1,0:T(8,128)(2,1)} %reshape.229, bf16[]{:T(256)} %constant.59.clone.1), kind=kCustom, calls=%fused_computation.17 | custom fusion | bytes 4194816 | tf_op jit(solution)/shard_map/scatter | solution.py:97
  33.9 11.7 %all-to-all-start = ((bf16[64,16,2048]{2,1,0:T(8,128)(2,1)}), bf16[64,16,2048]{2,1,0:T(8,128)(2,1)}, u32[]{:S(2)}, u32[]{:S(2)}) async-start(bf16[64,16,2048]{2,1,0:T(8,128)(2,1)} %bitcast.90), calls=%async_computation.1 | async-start | bytes 8388608 | tf_op jit(solution)/shard_map/all_to_all | solution.py:99
  45.9 0.5 fusion.26
  46.4 2.0 reshape.235
  48.4 2.3 pad_maximum_fusion.1
  50.8 1.8 copy.19
  52.6 1.8 copy.20
  54.4 1.9 fusion.1
  56.4 1.0 fusion
  57.5 1.2 fusion.17
  58.7 0.3 copy.24
  59.1 4.5 %fusion.29 = f32[1024,2048]{1,0:T(8,128)} fusion(bf16[256,2048]{1,0:T(8,128)(2,1)S(1)} %copy-done.3, bf16[32,8,8,128]{3,2,1,0:T(8,128)(2,1)S(1)} %bitcast.92), kind=kOutput, calls=%fused_computation.33 | convolution fusion | flops 1073741824 | bytes 9961472 | tf_op jit(solution)/shard_map/dot_general | solution.py:74
  63.6 76.6 %all-to-all-done = bf16[64,16,2048]{2,1,0:T(8,128)(2,1)} async-done(((bf16[64,16,2048]{2,1,0:T(8,128)(2,1)}), bf16[64,16,2048]{2,1,0:T(8,128)(2,1)}, u32[]{:S(2)}, u32[]{:S(2)}) %all-to-all-start) | async-done | bytes 4194336 | tf_op jit(solution)/shard_map/all_to_all | solution.py:99
  140.3 6.6 %fusion.3 = f32[1024,512]{1,0:T(8,128)} fusion(bf16[1024,2048]{1,0:T(8,128)(2,1)} %bitcast.15, bf16[1,2048,512]{2,1,0:T(8,128)(2,1)} %param.22), kind=kOutput, calls=%fused_computation.10 | convolution fusion | flops 2147483648 | bytes 8388608 | tf_op jit(solution)/shard_map/dot_general | solution.py:102
  146.8 10.4 %convolution_convert_fusion = bf16[1024,2048]{1,0:T(8,128)(2,1)} fusion(bf16[1,512,2048]{2,1,0:T(8,128)(2,1)S(1)} %copy-done, f32[1024,512]{1,0:T(8,128)} %fusion.3, bf16[1024,2048]{1,0:T(8,128)(2,1)} %bitcast.15, bf16[1,2048,512]{2,1,0:T(8,128)(2,1)} %param.21), kind=kOutput, calls=%fused_computation.6 | convolution fusion | flops 4302307328 | bytes 14680064 | tf_op jit(solution)/shard_map/dot_general | solution.py:104
  157.2 7.4 %all-to-all-start.1 = ((bf16[64,16,2048]{2,1,0:T(8,128)(2,1)}), bf16[64,16,2048]{2,1,0:T(8,128)(2,1)}, u32[]{:S(2)}, u32[]{:S(2)}) async-start(bf16[64,16,2048]{2,1,0:T(8,128)(2,1)} %bitcast.91), calls=%async_computation.2 | async-start | bytes 8388608 | tf_op jit(solution)/shard_map/all_to_all | solution.py:105
  164.7 94.8 %all-to-all-done.1 = bf16[64,16,2048]{2,1,0:T(8,128)(2,1)} async-done(((bf16[64,16,2048]{2,1,0:T(8,128)(2,1)}), bf16[64,16,2048]{2,1,0:T(8,128)(2,1)}, u32[]{:S(2)}, u32[]{:S(2)}) %all-to-all-start.1) | async-done | bytes 4194336 | tf_op jit(solution)/shard_map/all_to_all | solution.py:105
  259.5 8.0 %gather_fusion = bf16[512,2048]{1,0:T(8,128)(2,1)} fusion(bf16[1024,2048]{1,0:T(8,128)(2,1)} %bitcast.20, s32[1024]{0:T(1024)S(1)} %pad_clamp_fusion), kind=kCustom, calls=%fused_computation | custom fusion | bytes 4196352 | tf_op jit(solution)/shard_map/gather | solution.py:108
  267.4 4.8 %reshape.216 = f32[128,4,2048]{2,1,0:T(4,128)} reshape(bf16[512,2048]{1,0:T(8,128)(2,1)} %gather_fusion) | data formatting | bytes 6291456 | tf_op jit(solution)/shard_map/convert_element_type | solution.py:110
  272.3 6.2 %multiply_reduce_fusion = bf16[128,2048]{1,0:T(8,128)(2,1)} fusion(f32[128,4,2048]{2,1,0:T(4,128)} %reshape.216, f32[128,4]{1,0:T(8,128)S(1)} %copy.29), kind=kLoop, calls=%fused_computation.3 | loop fusion | flops 1835008 | bytes 4720640 | tf_op jit(solution)/shard_map/reduce_sum | solution.py:113
  278.5 2.7 convert_element_type.48
  (38 shorter events, 1.4 us)
Async XLA Ops:
  7.2 139.7 %copy-start = (bf16[1,512,2048]{2,1,0:T(8,128)(2,1)S(1)}, bf16[1,512,2048]{2,1,0:T(8,128)(2,1)}, u32[]{:S(2)}) copy-start(bf16[1,512,2048]{2,1,0:T(8,128)(2,1)} %param.23) | copy-start | bytes 6291460
  8.4 18.1 %copy-start.1 = (bf16[1024,64]{1,0:T(8,128)(2,1)}, bf16[1024,64]{1,0:T(8,128)(2,1)S(1)}, u32[]{:S(2)}) copy-start(bf16[1024,64]{1,0:T(8,128)(2,1)S(1)} %copy.17) | copy-start | bytes 393220
  9.6 16.9 %copy-start.2 = (bf16[1024,64]{1,0:T(8,128)(2,1)}, bf16[1024,64]{1,0:T(8,128)(2,1)S(1)}, u32[]{:S(2)}) copy-start(bf16[1024,64]{1,0:T(8,128)(2,1)S(1)} %copy.18) | copy-start | bytes 393220
  9.7 38.7 %collective-permute-start = (bf16[128,128]{1,0:T(8,128)(2,1)S(1)}, bf16[128,128]{1,0:T(8,128)(2,1)S(1)}, u32[]{:S(2)}, u32[]{:S(2)}) collective-permute-start(bf16[128,128]{1,0:T(8,128)(2,1)S(1)} %fusion.42), channel_id=1, source_target_pairs={{0,4},{4,8},{8,12},{12,16},{16,20},{20,24},{24,28},{28,32},{32,36}... | collective-permute-start | bytes 98312 | tf_op jit(solution)/shard_map/ppermute | solution.py:18
  33.9 106.4 %all-to-all-start = ((bf16[64,16,2048]{2,1,0:T(8,128)(2,1)}), bf16[64,16,2048]{2,1,0:T(8,128)(2,1)}, u32[]{:S(2)}, u32[]{:S(2)}) async-start(bf16[64,16,2048]{2,1,0:T(8,128)(2,1)} %bitcast.90), calls=%async_computation.1 | async-start | bytes 8388608 | tf_op jit(solution)/shard_map/all_to_all | solution.py:99
  45.6 232.9 %reduce-scatter.2.cloned.1.call-start = ((), (), s32[]{:S(2)}) async-start(), calls=%async_computation.3 | async-start | bytes 10485760 | tf_op jit(solution)/shard_map/reduce_scatter | solution.py:73
  48.4 7.9 %copy-start.6 = (f32[4]{0:T(128)S(1)}, f32[4]{0:T(128)}, u32[]{:S(2)}) copy-start(f32[4]{0:T(128)} %param.15) | copy-start | bytes 52
  54.4 3.1 %copy-start.4 = (bf16[8,128,128]{1,2,0:T(8,128)(2,1)S(1)}, bf16[8,128,128]{1,2,0:T(8,128)(2,1)}, u32[]{:S(2)}) copy-start(bf16[8,128,128]{1,2,0:T(8,128)(2,1)} %copy.19) | copy-start | bytes 786436
  54.4 3.1 %copy-start.5 = (bf16[8,128,128]{1,2,0:T(8,128)(2,1)S(1)}, bf16[8,128,128]{1,2,0:T(8,128)(2,1)}, u32[]{:S(2)}) copy-start(bf16[8,128,128]{1,2,0:T(8,128)(2,1)} %copy.20) | copy-start | bytes 786436
  57.5 1.6 copy-start.3
  157.2 7.4 %copy-start.7 = (f32[128,4]{0,1:T(4,128)S(1)}, f32[128,4]{0,1:T(4,128)}, u32[]{:S(2)}) copy-start(f32[128,4]{0,1:T(4,128)} %param.20) | copy-start | bytes 6148
  157.2 102.3 %all-to-all-start.1 = ((bf16[64,16,2048]{2,1,0:T(8,128)(2,1)}), bf16[64,16,2048]{2,1,0:T(8,128)(2,1)}, u32[]{:S(2)}, u32[]{:S(2)}) async-start(bf16[64,16,2048]{2,1,0:T(8,128)(2,1)} %bitcast.91), calls=%async_computation.2 | async-start | bytes 8388608 | tf_op jit(solution)/shard_map/all_to_all | solution.py:105
Sparse Core Ops, SparseCore 0:
  63.7 83.9 reduce-scatter.1
where the time goes:
time: 289 us; the launch traced here: 288 us
  waiting for transfers between devices  171 us (59%)
  local copies, waits for them, and re-layouts  36.3 us (13%)
  matrix products  24.6 us (9%)
  starting transfers between devices  23.8 us (8%)
  other arithmetic  17.6 us (6%)
  between operations  14.3 us (5%)
    all_to_all x1, waiting for transfers between devices, experts_part(): lax.all_to_all(result.reshape(arrived.shape), 'ep', split_axis=0, concat_...  94.8 us
    all_to_all x1, waiting for transfers between devices, experts_part(): lax.all_to_all(outgoing, 'ep', split_axis=0, concat_axis=0, tiled=True)  76.6 us
    all_to_all x1, starting transfers between devices, experts_part(): lax.all_to_all(outgoing, 'ep', split_axis=0, concat_axis=0, tiled=True)  11.7 us
    dot_general x1, matrix products, experts_part(): jnp.dot(act, down_weight[0], preferred_element_type=jnp.float32)  10.4 us
    gather x1, local copies, waits for them, and re-layouts, experts_part(): picked = came_back.reshape(targets * capacity, model_width)[slot_index]  7.95 us
    all_to_all x1, starting transfers between devices, experts_part(): lax.all_to_all(result.reshape(arrived.shape), 'ep', split_axis=0, concat_...  7.35 us
    scatter x1, local copies, waits for them, and re-layouts, experts_part(): jnp.zeros((targets * capacity, model_width), jnp.bfloat16).at[slot_index]  7.24 us
    dot_general x1, matrix products, experts_part(): jnp.dot(flat_rows, up_weight[0], preferred_element_type=jnp.float32)  6.57 us
  transfers between devices with their start and end apart: 4, of which 2 were waited for; matrix products, arithmetic and copies ran while one was open for 25% of the time, Pallas kernels for 0%

commit v1 on v0

v1 whole, which is shorter than its diff:
```python
import functools

import jax
import jax.numpy as jnp
from jax import lax
from jax.experimental import pallas as pl
from jax.experimental.pallas import tpu as pltpu
from jax.sharding import PartitionSpec as P

MESH = pl.DeviceIdType.MESH
HEAD_DIM = 64
WINDOW = 128
CAP = 16
EPSILON = 1e-05
NEGATIVE = -1e30
PIECES = 2


def clamped_unit(gate_pre, up_pre):
    gate_cut = jnp.minimum(gate_pre, 7.0)
    up_cut = jnp.clip(up_pre, -7.0, 7.0)
    return gate_cut * jax.nn.sigmoid(1.702 * gate_cut) * (up_cut + 1.0)


def bytes_wait(ref, sem):
    pltpu.make_async_copy(ref, ref, sem).wait()


def kernel(
    Z,
    L,
    X,
    S,
    x_ref,
    gain_ref,
    routes_ref,
    rweight_ref,
    q_ref,
    k_ref,
    v_ref,
    sink_ref,
    ow_hbm,
    gw_hbm,
    uw_hbm,
    dw_hbm,
    att_ref,
    out_ref,
    ag,
    tab,
    pick,
    spread,
    disp,
    recv,
    res,
    ret,
    rs_out,
    rs_in,
    gw,
    uw,
    dw,
    wall,
    kv2,
    heads,
    hall,
    ld_sem,
    tab_send,
    tab_recv,
    z_send,
    z_recv,
    y_send,
    y_recv,
    r_send,
    r_recv,
    rs_send,
    rs_recv,
    w_send,
    w_recv,
    h_send,
    h_recv,
    halo_send,
    halo_recv,
):
    T, D = x_ref.shape
    DS = D // S
    H = Z // 2
    U = (H - 1) * S + S // 2
    EP = Z * L
    rows = q_ref.shape[0]
    per_x = rows // X
    ep = lax.axis_index("ep")
    x = lax.axis_index("tp")
    z = ep // L
    me = lax.rem(ep, L)

    def dev_z(step):
        return (lax.rem(z + step + Z, Z) * L + me, x)

    def dev_l(l):
        return (z * L + l, x)

    def dev_x(step):
        return (ep, lax.rem(x + step, X))

    right_ep = (lax.rem(ep + 1, EP), x)
    left_ep = (lax.rem(ep + EP - 1, EP), x)

    loads = [
        pltpu.make_async_copy(ow_hbm, wall.at[x], ld_sem.at[0]),
        pltpu.make_async_copy(gw_hbm.at[0], gw, ld_sem.at[1]),
        pltpu.make_async_copy(uw_hbm.at[0], uw, ld_sem.at[2]),
        pltpu.make_async_copy(dw_hbm.at[0], dw, ld_sem.at[3]),
    ]
    barrier = pltpu.get_barrier_semaphore()
    met = [dev_z(r) for r in range(1, Z)]
    met += [dev_l(lax.rem(me + r, L)) for r in range(1, L)]
    met += [dev_x(r) for r in range(1, X)]
    met += [right_ep, left_ep]
    for target in met:
        pl.semaphore_signal(barrier, inc=1, device_id=target, device_id_type=MESH)
    for load in loads:
        load.start()

    values32 = x_ref[...].astype(jnp.float32)
    scale = lax.rsqrt(jnp.mean(values32 * values32, axis=-1, keepdims=True) + EPSILON)
    normed = (values32 * scale * gain_ref[...]).astype(jnp.bfloat16)
    for f in range(S):
        ag[0, f] = normed[:, f * DS : (f + 1) * DS]
    tab[0, 0:4] = routes_ref[...].astype(jnp.float32).T
    tab[0, 4:8] = rweight_ref[...].T
    kv2[0, WINDOW:] = jnp.concatenate([k_ref[...], k_ref[...]], axis=1)
    kv2[1, WINDOW:] = jnp.concatenate([v_ref[...], v_ref[...]], axis=1)

    pl.semaphore_wait(barrier, len(met))

    def tab_copy(r):
        return pltpu.make_async_remote_copy(
            src_ref=tab.at[0],
            dst_ref=tab.at[Z - r],
            send_sem=tab_send,
            recv_sem=tab_recv.at[Z - r],
            device_id=dev_z(r),
            device_id_type=MESH,
        )

    for r in range(1, Z):
        tab_copy(r).start()

    def ring_copy(direction, u):
        hop, i = u // S + 1, lax.rem(u, S)
        if direction == 0:
            f, src, dst, target = i, lax.rem(Z - hop + 1, Z), Z - hop, dev_z(1)
        else:
            f, src, dst, target = S - 1 - i, hop - 1, hop, dev_z(-1)
        return pltpu.make_async_remote_copy(
            src_ref=ag.at[src, f],
            dst_ref=ag.at[dst, f],
            send_sem=z_send.at[direction],
            recv_sem=z_recv.at[direction, u],
            device_id=target,
            device_id_type=MESH,
        )

    for u in range(min(S, U)):
        ring_copy(0, u).start()
        ring_copy(1, u).start()

    halo = pltpu.make_async_remote_copy(
        src_ref=kv2.at[:, pl.ds(rows, WINDOW)],
        dst_ref=kv2.at[:, pl.ds(0, WINDOW)],
        send_sem=halo_send,
        recv_sem=halo_recv,
        device_id=right_ep,
        device_id_type=MESH,
    )
    halo.start()

    def make_slots(o):
        table = tab[o]
        expert = (lax.broadcasted_iota(jnp.int32, (L, T), 0) + z * L).astype(jnp.float32)
        named = jnp.zeros((L, T), jnp.float32)
        weight = jnp.zeros((L, T), jnp.float32)
        for k in range(4):
            hit = table[k : k + 1, :] == expert
            named = named + jnp.where(hit, 1.0, 0.0)
            weight = weight + jnp.where(hit, table[4 + k : 5 + k, :], 0.0)
        before = (
            lax.broadcasted_iota(jnp.int32, (T, T), 0) < lax.broadcasted_iota(jnp.int32, (T, T), 1)
        ).astype(jnp.float32)
        rank = jnp.dot(named, before, preferred_element_type=jnp.float32)
        rank = jnp.where(named > 0.5, rank, -1.0)
        slot = lax.broadcasted_iota(jnp.int32, (CAP, T), 0).astype(jnp.float32)
        hits = jnp.concatenate(
            [jnp.where(rank[l : l + 1, :] == slot, 1.0, 0.0) for l in range(L)], axis=0
        )
        weights = jnp.concatenate(
            [jnp.where(rank[l : l + 1, :] == slot, weight[l : l + 1, :], 0.0) for l in range(L)],
            axis=0,
        )
        pick[o] = hits.astype(jnp.bfloat16)
        turned = weights.T
        high = turned.astype(jnp.bfloat16)
        spread[o, 0] = high
        spread[o, 1] = (turned - high.astype(jnp.float32)).astype(jnp.bfloat16)

    def dispatch(o, f):
        chosen = jnp.dot(pick[o], ag[o, f], preferred_element_type=jnp.float32)
        disp[o, f] = chosen.astype(jnp.bfloat16).reshape(L, CAP, DS)
        recv[o, f, me] = disp[o, f, me]
        for r in range(1, L):
            l = lax.rem(me + r, L)
            pltpu.make_async_remote_copy(
                src_ref=disp.at[o, f, l],
                dst_ref=recv.at[o, f, me],
                send_sem=y_send,
                recv_sem=y_recv.at[o],
                device_id=dev_l(l),
                device_id_type=MESH,
            ).start()

    def give_back(o, f):
        for r in range(1, L):
            l = lax.rem(me + r, L)
            pltpu.make_async_remote_copy(
                src_ref=res.at[o, f, l],
                dst_ref=ret.at[o, f, me],
                send_sem=r_send,
                recv_sem=r_recv.at[o, f],
                device_id=dev_l(l),
                device_id_type=MESH,
            ).start()

    def expert(o):
        bytes_wait(disp.at[o, :, pl.ds(0, L - 1)], y_recv.at[o])
        gate_pre = jnp.zeros((L * CAP, gw.shape[1]), jnp.float32)
        up_pre = jnp.zeros((L * CAP, gw.shape[1]), jnp.float32)
        for f in range(S):
            block = recv[o, f].reshape(L * CAP, DS)
            cut = slice(f * DS, (f + 1) * DS)
            gate_pre += jnp.dot(block, gw[cut, :], preferred_element_type=jnp.float32)
            up_pre += jnp.dot(block, uw[cut, :], preferred_element_type=jnp.float32)
        act = clamped_unit(gate_pre, up_pre).astype(jnp.bfloat16)
        for f in range(S):
            cut = slice(f * DS, (f + 1) * DS)
            result = jnp.dot(act, dw[:, cut], preferred_element_type=jnp.float32)
            res[o, f] = result.astype(jnp.bfloat16).reshape(L, CAP, DS)
            ret[o, f, me] = res[o, f, me]

    def combine(o, f):
        bytes_wait(res.at[o, f, pl.ds(0, L - 1)], r_recv.at[o, f])
        block = ret[o, f].reshape(L * CAP, DS)
        return jnp.dot(spread[o, 0], block, preferred_element_type=jnp.float32) + jnp.dot(
            spread[o, 1], block, preferred_element_type=jnp.float32
        )

    def job_offset(k):
        h = (k + 1) // 2
        odd = lax.rem(k, 2)
        return odd * (Z - h) + (1 - odd) * h

    make_slots(0)
    for f in range(S):
        dispatch(0, f)

    loads[0].wait()

    def weight_copy(r):
        return pltpu.make_async_remote_copy(
            src_ref=wall.at[x],
            dst_ref=wall.at[x],
            send_sem=w_send,
            recv_sem=w_recv,
            device_id=dev_x(r),
            device_id_type=MESH,
        )

    for r in range(1, X):
        weight_copy(r).start()

    blocks = rows // WINDOW

    def attend(step, carry):
        b = blocks - 1 - step

        @pl.when(b == 0)
        def _():
            halo.wait_recv()

        first = pl.multiple_of(b * WINDOW, WINDOW)
        keys = kv2[0, pl.ds(first, 2 * WINDOW), :]
        vals = kv2[1, pl.ds(first, 2 * WINDOW), :]
        qs = lax.broadcasted_iota(jnp.int32, (WINDOW, 2 * WINDOW), 0)
        ks = lax.broadcasted_iota(jnp.int32, (WINDOW, 2 * WINDOW), 1)
        lowest = jnp.where((ep == 0) & (b == 0), WINDOW, 0)
        valid = (ks > qs) & (ks <= qs + WINDOW) & (ks >= lowest)
        lower = lax.broadcasted_iota(jnp.int32, (WINDOW, 2 * HEAD_DIM), 1) < HEAD_DIM
        for pair in range(2):
            cut = slice(pair * 2 * HEAD_DIM, (pair + 1) * 2 * HEAD_DIM)
            both = q_ref[pl.ds(first, WINDOW), cut]
            halves = []
            for half in range(2):
                keep = lower if half == 0 else jnp.logical_not(lower)
                mine = jnp.where(keep, both, jnp.zeros_like(both))
                scores = lax.dot_general(
                    mine, keys, (((1,), (1,)), ((), ())), preferred_element_type=jnp.float32
                ) * HEAD_DIM ** (-0.5)
                scores = jnp.where(valid, scores, NEGATIVE)
                sink = sink_ref[2 * pair + half]
                maxima = jnp.maximum(jnp.max(scores, axis=-1, keepdims=True), sink)
                powers = jnp.exp(scores - maxima)
                total = jnp.sum(powers, axis=-1, keepdims=True) + jnp.exp(sink - maxima)
                weights = (powers / total).astype(jnp.bfloat16)
                halves.append(jnp.dot(weights, vals, preferred_element_type=jnp.float32))
            done = jnp.where(lower, halves[0], halves[1]).astype(jnp.bfloat16)
            heads[
                b * WINDOW // per_x, pl.ds(pl.multiple_of(lax.rem(b * WINDOW, per_x), WINDOW), WINDOW), cut
            ] = done
        return carry

    lax.fori_loop(0, blocks, attend, 0)
    hall[x] = heads[x]
    for r in range(1, X):
        pltpu.make_async_remote_copy(
            src_ref=heads.at[lax.rem(x + r, X)],
            dst_ref=hall.at[x],
            send_sem=h_send,
            recv_sem=h_recv,
            device_id=dev_x(r),
            device_id_type=MESH,
        ).start()

    for load in loads[1:]:
        load.wait()

    def spread_step(u, carry):
        hop, i = u // S + 1, lax.rem(u, S)
        for direction in range(2):
            ring_copy(direction, u).wait_recv()

            @pl.when(u + S < U)
            def _():
                ring_copy(direction, u + S).start()

        @pl.when(i == 0)
        def _():
            bytes_wait(tab.at[0], tab_recv.at[hop])
            make_slots(hop)

            @pl.when(hop < H)
            def _():
                bytes_wait(tab.at[0], tab_recv.at[Z - hop])
                make_slots(Z - hop)

        dispatch(Z - hop, i)
        dispatch(hop, S - 1 - i)
        half = S // 2
        k = jnp.where(u == half, 0, u // half - 2)

        @pl.when((lax.rem(u, half) == 0) & ((u == half) | (k >= 1)))
        def _():
            o = job_offset(k)
            expert(o)

            @pl.when(u == half)
            def _():
                for f in range(S):
                    give_back(0, f)

        return carry

    lax.fori_loop(0, U, spread_step, 0)

    def back_unit(u):
        hop, i = u // S + 1, lax.rem(u, S)
        give_back(Z - hop, i)
        give_back(hop, S - 1 - i)

    first_late = max(1, Z - 3)

    def late_job(k, carry):
        expert(job_offset(k))

        @pl.when(k == Z - 2)
        def _():
            back_unit(0)

        return carry

    if U <= S // 2:
        expert(0)
        for f in range(S):
            give_back(0, f)
    lax.fori_loop(first_late, Z, late_job, 0)

    ahead = 3
    for j in range(ahead):
        if U - 1 - j >= 1:
            back_unit(U - 1 - j)

    def rs_copy(direction, u):
        return pltpu.make_async_remote_copy(
            src_ref=rs_out.at[direction, u],
            dst_ref=rs_in.at[direction, u],
            send_sem=rs_send.at[direction],
            recv_sem=rs_recv.at[direction, u],
            device_id=dev_z(1 if direction == 0 else -1),
            device_id_type=MESH,
        )

    for direction in range(2):
        for u in range(U, U + S):
            rs_in[direction, u] = jnp.zeros((T, DS), jnp.bfloat16)

    def gather_step(v, carry):
        u = U - 1 - v
        hop, i = u // S + 1, lax.rem(u, S)

        @pl.when(u - ahead >= 1)
        def _():
            back_unit(u - ahead)

        for direction in range(2):
            o, f = (hop, S - 1 - i) if direction == 0 else (Z - hop, i)
            value = combine(o, f)

            @pl.when(u + S < U)
            def _():
                rs_copy(direction, u + S).wait_recv()

            value = value + rs_in[direction, u + S].astype(jnp.float32)
            rs_out[direction, u] = value.astype(jnp.bfloat16)
            rs_copy(direction, u).start()

        @pl.when(v == 1)
        def _():
            bytes_wait(wall.at[pl.ds(0, X - 1)], w_recv)
            bytes_wait(hall.at[pl.ds(0, X - 1)], h_recv)
            wide = att_ref.shape[1] // 4
            for n in range(4):
                cut = slice(n * wide, (n + 1) * wide)
                total = jnp.dot(hall[0], wall[0, :, cut], preferred_element_type=jnp.float32)
                for s in range(1, X):
                    total += jnp.dot(hall[s], wall[s, :, cut], preferred_element_type=jnp.float32)
                att_ref[:, cut] = total.astype(jnp.bfloat16)

        return carry

    lax.fori_loop(0, U, gather_step, 0)

    for f in range(S):
        value = combine(0, f)
        rs_copy(0, S - 1 - f).wait_recv()
        rs_copy(1, f).wait_recv()
        value = value + rs_in[0, S - 1 - f].astype(jnp.float32) + rs_in[1, f].astype(jnp.float32)
        out_ref[:, f * DS : (f + 1) * DS] = value.astype(jnp.bfloat16)

    bytes_wait(tab.at[pl.ds(0, Z - 1)], tab_send)
    for direction in range(2):
        bytes_wait(rs_in.at[direction, pl.ds(0, U)], z_send.at[direction])
        bytes_wait(rs_in.at[direction, pl.ds(0, U)], rs_send.at[direction])
    bytes_wait(disp.at[:, :, pl.ds(0, L - 1)], y_send)
    bytes_wait(res.at[:, :, pl.ds(0, L - 1)], r_send)
    bytes_wait(wall.at[pl.ds(0, X - 1)], w_send)
    bytes_wait(heads.at[pl.ds(0, X - 1)], h_send)
    halo.wait_send()


def on_device(
    Z,
    L,
    X,
    queries,
    head_keys,
    head_values,
    sink_logits,
    out_weight,
    moe_input,
    norm_gain,
    routes,
    route_weight,
    gate_weight,
    up_weight,
    down_weight,
):
    S = PIECES
    T, D = moe_input.shape
    DS = D // S
    FF = gate_weight.shape[2]
    rows, cols = queries.shape
    H = Z // 2
    U = (H - 1) * S + S // 2
    slots = L * CAP
    bf16, f32 = jnp.bfloat16, jnp.float32
    vmem = pl.BlockSpec(memory_space=pltpu.VMEM)
    hbm = pl.BlockSpec(memory_space=pl.ANY)
    dma = pltpu.SemaphoreType.DMA
    attention_out, routed_out = pl.pallas_call(
        functools.partial(kernel, Z, L, X, S),
        out_shape=(
            jax.ShapeDtypeStruct((rows // X, D), bf16),
            jax.ShapeDtypeStruct((T, D), bf16),
        ),
        in_specs=[vmem] * 7 + [pl.BlockSpec(memory_space=pltpu.SMEM)] + [hbm] * 4,
        out_specs=(vmem, vmem),
        scratch_shapes=[
            pltpu.VMEM((Z, S, T, DS), bf16),
            pltpu.VMEM((Z, 8, T), f32),
            pltpu.VMEM((Z, slots, T), bf16),
            pltpu.VMEM((Z, 2, T, slots), bf16),
            pltpu.VMEM((Z, S, L, CAP, DS), bf16),
            pltpu.VMEM((Z, S, L, CAP, DS), bf16),
            pltpu.VMEM((Z, S, L, CAP, DS), bf16),
            pltpu.VMEM((Z, S, L, CAP, DS), bf16),
            pltpu.VMEM((2, U, T, DS), bf16),
            pltpu.VMEM((2, U + S, T, DS), bf16),
            pltpu.VMEM((D, FF), bf16),
            pltpu.VMEM((D, FF), bf16),
            pltpu.VMEM((FF, D), bf16),
            pltpu.VMEM((X, cols, D), bf16),
            pltpu.VMEM((2, rows + WINDOW, 2 * HEAD_DIM), bf16),
            pltpu.VMEM((X, rows // X, cols), bf16),
            pltpu.VMEM((X, rows // X, cols), bf16),
            dma((4,)),
            dma,
            dma((Z,)),
            dma((2,)),
            dma((2, U)),
            dma,
            dma((Z,)),
            dma,
            dma((Z, S)),
            dma((2,)),
            dma((2, U)),
            dma,
            dma,
            dma,
            dma,
            dma,
            dma,
        ],
        compiler_params=pltpu.CompilerParams(
            collective_id=0, has_side_effects=True, vmem_limit_bytes=60 * 1024 * 1024
        ),
    )(
        moe_input,
        norm_gain.reshape(1, D),
        routes,
        route_weight,
        queries,
        head_keys,
        head_values,
        sink_logits,
        out_weight,
        gate_weight,
        up_weight,
        down_weight,
    )
    return (attention_out, routed_out)


def solution(mesh, layer=8):
    X = mesh.shape["tp"]
    Z = mesh.shape["ep"] // layer
    placed = (
        P("ep", "tp"),
        P("ep", "tp"),
        P("ep", "tp"),
        P("tp"),
        P("tp", None),
        P(("ep", "tp"), None),
        P(),
        P(("ep", "tp"), None),
        P(("ep", "tp"), None),
        P("ep", None, None),
        P("ep", None, None),
        P("ep", None, None),
    )
    return jax.shard_map(
        functools.partial(on_device, Z, layer, X),
        mesh=mesh,
        in_specs=placed,
        out_specs=(P(("ep", "tp"), None), P(("ep", "tp"), None)),
        check_vma=False,
    )
```

time: 289 us -> 135 us (0.47)
  waiting for transfers between devices: 171 us -> 0 us
  Pallas kernels: 0 us -> 125 us
  local copies, waits for them, and re-layouts: 36.3 us -> 9.45 us
  matrix products: 24.6 us -> 0 us
  starting transfers between devices: 23.8 us -> 0 us
  other arithmetic: 17.6 us -> 0 us
  between operations: 14.3 us -> 0.65 us
    all_to_all x2 -> x0, waiting for transfers between devices: 171 us -> none  [the longest x1 94.8 us: experts_part(): lax.all_to_all(result.reshape(arrived.shape), 'ep', split_axis=0, concat_...]
    pallas_call x0 -> x1, Pallas kernels: none -> 125 us  [on_device(): pl.pallas_call(functools.partial(kernel, Z, L, X, S), out_shape=(jax.Shap...]
    dot_general x5 -> x0, matrix products: 24.6 us -> none  [the longest x1 10.4 us: experts_part(): jnp.dot(act, down_weight[0], preferred_element_type=jnp.float32)]
    all_to_all x2 -> x0, starting transfers between devices: 19 us -> none  [the longest x1 11.7 us: experts_part(): lax.all_to_all(outgoing, 'ep', split_axis=0, concat_axis=0, tiled=True)]
    reduce_sum x4 -> x0, other arithmetic: 8.58 us -> none  [the longest x1 6.2 us: experts_part(): return jnp.sum(weighted, axis=1).astype(jnp.bfloat16)]
    gather x1 -> x0, local copies, waits for them, and re-layouts: 7.95 us -> none  [experts_part(): picked = came_back.reshape(targets * capacity, model_width)[slot_index]]
    reshape x3 -> x0, local copies, waits for them, and re-layouts: 7.54 us -> none  [the longest x1 3.96 us: experts_part(): copies = jnp.repeat(normed, choice_count, axis=0)]
    scatter x1 -> x0, local copies, waits for them, and re-layouts: 7.24 us -> none  [experts_part(): jnp.zeros((targets * capacity, model_width), jnp.bfloat16).at[slot_index]]
  transfers between devices with their start and end apart: 4 -> 0, of which waited for: 2 -> 0; matrix products, arithmetic and copies ran while one was open for 25% -> 0% of each run, Pallas kernels for 0% -> 0%
where the time goes in v1:
time: 135 us
  Pallas kernels  125 us (93%)
  local copies, waits for them, and re-layouts  9.45 us (7%)
    pallas_call x1, Pallas kernels, on_device(): pl.pallas_call(functools.partial(kernel, Z, L, X, S), out_shape=(jax.Shap...  125 us
    unnamed x8, local copies, waits for them, and re-layouts  9.45 us

profile of v1, /device:TPU:1, one launch (start us, length us, event | category | flops | bytes accessed | tf_op | source)
XLA Modules:
  0.0 134.9 jit_solution(6029845859179072058)
XLA Ops:
  0.6 1.4 %copy.14.routes_ref = s32[128,4]{1,0:T(8,128)} copy(s32[128,4]{0,1:T(4,128)} %param.19) | data formatting | bytes 4096 | tf_op args[7]
  2.0 1.4 %copy.15.rweight_ref = f32[128,4]{1,0:T(8,128)} copy(f32[128,4]{0,1:T(4,128)} %param.20) | data formatting | bytes 4096 | tf_op args[8]
  3.4 1.7 %copy.16.k_ref = bf16[1024,64]{1,0:T(8,128)(2,1)} copy(bf16[1024,64]{0,1:T(8,128)(2,1)} %param.13) | data formatting | bytes 262144 | tf_op args[1]
  5.2 1.7 %copy.17.v_ref = bf16[1024,64]{1,0:T(8,128)(2,1)} copy(bf16[1024,64]{0,1:T(8,128)(2,1)} %param.14) | data formatting | bytes 262144 | tf_op args[2]
  6.9 124.8 %shard_map.131 = (bf16[256,2048]{1,0:T(8,128)(2,1)}, bf16[128,2048]{1,0:T(8,128)(2,1)}) custom-call(bf16[128,2048]{1,0:T(8,128)(2,1)} %x_ref.1, f32[1,2048]{1,0:T(1,128)} %bitcast.1, s32[128,4]{1,0:T(8,128)} %copy.14.routes_ref, f32[128,4]{1,0:T(8,128)} %copy.15.rweight_ref, bf16[1024,256]{1,0:T(8,128)(2,1)} %q_ref.1, bf16[1024,64]{1,0:T(8,128)(2,1)} %copy.16.k_ref, ...), custom_call_target="tpu_custom_call" | custom-call | tf_op jit(solution)/shard_map/pallas_call | solution.py:496
  131.7 0.0 copy-start
  131.7 2.4 %copy.20 = bf16[256,2048]{1,0:T(8,128)(2,1)} copy(bf16[256,2048]{1,0:T(8,128)(2,1)} %get-tuple-element.4) | data formatting | bytes 2097152
  134.1 0.0 copy-done
  134.1 0.8 copy.21
Async XLA Ops:
  131.7 2.4 %copy-start = (bf16[128,2048]{1,0:T(8,128)(2,1)S(1)}, bf16[128,2048]{1,0:T(8,128)(2,1)}, u32[]{:S(2)}) copy-start(bf16[128,2048]{1,0:T(8,128)(2,1)} %get-tuple-element.5) | copy-start | bytes 1572868

commit v2 on v1

--- a/solution.py
+++ b/solution.py
@@ -13,7 +13,10 @@
 CAP = 16
 EPSILON = 1e-05
 NEGATIVE = -1e30
-PIECES = 2
+PIECES = 4
+AHEAD = 4
+EARLY = 3
+FILL = 1
 
 
 def clamped_unit(gate_pre, up_pre):
@@ -23,6 +26,8 @@
 
 
 def bytes_wait(ref, sem):
+    if 0 in ref.shape:
+        return
     pltpu.make_async_copy(ref, ref, sem).wait()
 
 
@@ -111,7 +116,7 @@
         pltpu.make_async_copy(dw_hbm.at[0], dw, ld_sem.at[3]),
     ]
     barrier = pltpu.get_barrier_semaphore()
-    met = [dev_z(r) for r in range(1, Z)]
+    met = [dev_z(1), dev_z(-1)]
     met += [dev_l(lax.rem(me + r, L)) for r in range(1, L)]
     met += [dev_x(r) for r in range(1, X)]
     met += [right_ep, left_ep]
@@ -125,25 +130,42 @@
     normed = (values32 * scale * gain_ref[...]).astype(jnp.bfloat16)
     for f in range(S):
         ag[0, f] = normed[:, f * DS : (f + 1) * DS]
-    tab[0, 0:4] = routes_ref[...].astype(jnp.float32).T
-    tab[0, 4:8] = rweight_ref[...].T
-    kv2[0, WINDOW:] = jnp.concatenate([k_ref[...], k_ref[...]], axis=1)
-    kv2[1, WINDOW:] = jnp.concatenate([v_ref[...], v_ref[...]], axis=1)
+    tab[0, 0:4] = routes_ref[...].astype(jnp.float32)
+    tab[0, 4:8] = rweight_ref[...]
+    for half in range(2):
+        cut = slice(half * HEAD_DIM, (half + 1) * HEAD_DIM)
+        kv2[0, cut, WINDOW:] = k_ref[...]
+        kv2[1, cut, WINDOW:] = v_ref[...]
 
     pl.semaphore_wait(barrier, len(met))
 
-    def tab_copy(r):
+    halo = pltpu.make_async_remote_copy(
+        src_ref=kv2.at[:, :, pl.ds(rows, WINDOW)],
+        dst_ref=kv2.at[:, :, pl.ds(0, WINDOW)],
+        send_sem=halo_send,
+        recv_sem=halo_recv,
+        device_id=right_ep,
+        device_id_type=MESH,
+    )
+    halo.start()
+
+    def tab_copy(direction, hop):
+        if direction == 0:
+            src, dst, target = lax.rem(Z - hop + 1, Z), Z - hop, dev_z(1)
+        else:
+            src, dst, target = hop - 1, hop, dev_z(-1)
         return pltpu.make_async_remote_copy(
-            src_ref=tab.at[0],
-            dst_ref=tab.at[Z - r],
+            src_ref=tab.at[src],
+            dst_ref=tab.at[dst],
             send_sem=tab_send,
-            recv_sem=tab_recv.at[Z - r],
-            device_id=dev_z(r),
+            recv_sem=tab_recv.at[dst],
+            device_id=target,
             device_id_type=MESH,
         )
 
-    for r in range(1, Z):
-        tab_copy(r).start()
+    tab_copy(0, 1).start()
+    if H > 1:
+        tab_copy(1, 1).start()
 
     def ring_copy(direction, u):
         hop, i = u // S + 1, lax.rem(u, S)
@@ -163,16 +185,6 @@
     for u in range(min(S, U)):
         ring_copy(0, u).start()
         ring_copy(1, u).start()
-
-    halo = pltpu.make_async_remote_copy(
-        src_ref=kv2.at[:, pl.ds(rows, WINDOW)],
-        dst_ref=kv2.at[:, pl.ds(0, WINDOW)],
-        send_sem=halo_send,
-        recv_sem=halo_recv,
-        device_id=right_ep,
-        device_id_type=MESH,
-    )
-    halo.start()
 
     def make_slots(o):
         table = tab[o]
@@ -258,7 +270,7 @@
         return odd * (Z - h) + (1 - odd) * h
 
     make_slots(0)
-    for f in range(S):
+    for f in range(EARLY):
         dispatch(0, f)
 
     loads[0].wait()
@@ -280,14 +292,9 @@
 
     def attend(step, carry):
         b = blocks - 1 - step
-
-        @pl.when(b == 0)
-        def _():
-            halo.wait_recv()
-
         first = pl.multiple_of(b * WINDOW, WINDOW)
-        keys = kv2[0, pl.ds(first, 2 * WINDOW), :]
-        vals = kv2[1, pl.ds(first, 2 * WINDOW), :]
+        keys = kv2[0, :, pl.ds(first, 2 * WINDOW)]
+        vals = kv2[1, :, pl.ds(first, 2 * WINDOW)]
         qs = lax.broadcasted_iota(jnp.int32, (WINDOW, 2 * WINDOW), 0)
         ks = lax.broadcasted_iota(jnp.int32, (WINDOW, 2 * WINDOW), 1)
         lowest = jnp.where((ep == 0) & (b == 0), WINDOW, 0)
@@ -300,25 +307,34 @@
             for half in range(2):
                 keep = lower if half == 0 else jnp.logical_not(lower)
                 mine = jnp.where(keep, both, jnp.zeros_like(both))
-                scores = lax.dot_general(
-                    mine, keys, (((1,), (1,)), ((), ())), preferred_element_type=jnp.float32
-                ) * HEAD_DIM ** (-0.5)
+                scores = jnp.dot(mine, keys, preferred_element_type=jnp.float32) * HEAD_DIM ** (-0.5)
                 scores = jnp.where(valid, scores, NEGATIVE)
                 sink = sink_ref[2 * pair + half]
                 maxima = jnp.maximum(jnp.max(scores, axis=-1, keepdims=True), sink)
                 powers = jnp.exp(scores - maxima)
                 total = jnp.sum(powers, axis=-1, keepdims=True) + jnp.exp(sink - maxima)
                 weights = (powers / total).astype(jnp.bfloat16)
-                halves.append(jnp.dot(weights, vals, preferred_element_type=jnp.float32))
+                halves.append(
+                    lax.dot_general(
+                        weights, vals, (((1,), (1,)), ((), ())), preferred_element_type=jnp.float32
+                    )
+                )
             done = jnp.where(lower, halves[0], halves[1]).astype(jnp.bfloat16)
             heads[
                 b * WINDOW // per_x, pl.ds(pl.multiple_of(lax.rem(b * WINDOW, per_x), WINDOW), WINDOW), cut
             ] = done
         return carry
 
-    lax.fori_loop(0, blocks, attend, 0)
-    hall[x] = heads[x]
-    for r in range(1, X):
+    lax.fori_loop(0, blocks - 1, attend, 0)
+
+    def finish_heads():
+        halo.wait_recv()
+        attend(blocks - 1, 0)
+        hall[x] = heads[x]
+        for r in range(1, X):
+            send_heads(r)
+
+    def send_heads(r):
         pltpu.make_async_remote_copy(
             src_ref=heads.at[lax.rem(x + r, X)],
             dst_ref=hall.at[x],
@@ -342,28 +358,32 @@
 
         @pl.when(i == 0)
         def _():
-            bytes_wait(tab.at[0], tab_recv.at[hop])
-            make_slots(hop)
+            bytes_wait(tab.at[0], tab_recv.at[Z - hop])
 
             @pl.when(hop < H)
             def _():
-                bytes_wait(tab.at[0], tab_recv.at[Z - hop])
-                make_slots(Z - hop)
+                tab_copy(0, hop + 1).start()
+                bytes_wait(tab.at[0], tab_recv.at[hop])
+                make_slots(hop)
+
+            @pl.when(hop < H - 1)
+            def _():
+                tab_copy(1, hop + 1).start()
+
+            make_slots(Z - hop)
 
         dispatch(Z - hop, i)
         dispatch(hop, S - 1 - i)
         half = S // 2
-        k = jnp.where(u == half, 0, u // half - 2)
-
-        @pl.when((lax.rem(u, half) == 0) & ((u == half) | (k >= 1)))
-        def _():
-            o = job_offset(k)
-            expert(o)
-
-            @pl.when(u == half)
-            def _():
-                for f in range(S):
-                    give_back(0, f)
+        k = u // half - 2
+
+        @pl.when((lax.rem(u, half) == 0) & (k >= 1))
+        def _():
+            expert(job_offset(k))
+
+        @pl.when(u == S - 1)
+        def _():
+            finish_heads()
 
         return carry
 
@@ -378,23 +398,17 @@
 
     def late_job(k, carry):
         expert(job_offset(k))
-
-        @pl.when(k == Z - 2)
-        def _():
-            back_unit(0)
-
         return carry
 
-    if U <= S // 2:
-        expert(0)
-        for f in range(S):
-            give_back(0, f)
+    for f in range(EARLY, S):
+        dispatch(0, f)
+    for u in range(FILL):
+        back_unit(u)
     lax.fori_loop(first_late, Z, late_job, 0)
 
-    ahead = 3
+    ahead = min(AHEAD, U)
     for j in range(ahead):
-        if U - 1 - j >= 1:
-            back_unit(U - 1 - j)
+        back_unit(U - 1 - j)
 
     def rs_copy(direction, u):
         return pltpu.make_async_remote_copy(
@@ -414,9 +428,18 @@
         u = U - 1 - v
         hop, i = u // S + 1, lax.rem(u, S)
 
-        @pl.when(u - ahead >= 1)
+        @pl.when(u - ahead >= FILL)
         def _():
             back_unit(u - ahead)
+
+        @pl.when(v == 1)
+        def _():
+            expert(0)
+
+        @pl.when(u == ahead + FILL - 1)
+        def _():
+            for f in range(S):
+                give_back(0, f)
 
         for direction in range(2):
             o, f = (hop, S - 1 - i) if direction == 0 else (Z - hop, i)
@@ -430,17 +453,21 @@
             rs_out[direction, u] = value.astype(jnp.bfloat16)
             rs_copy(direction, u).start()
 
-        @pl.when(v == 1)
+        first = U // 2
+        wide = att_ref.shape[1] // 4
+
+        @pl.when(v == first)
         def _():
             bytes_wait(wall.at[pl.ds(0, X - 1)], w_recv)
             bytes_wait(hall.at[pl.ds(0, X - 1)], h_recv)
-            wide = att_ref.shape[1] // 4
-            for n in range(4):
-                cut = slice(n * wide, (n + 1) * wide)
-                total = jnp.dot(hall[0], wall[0, :, cut], preferred_element_type=jnp.float32)
-                for s in range(1, X):
-                    total += jnp.dot(hall[s], wall[s, :, cut], preferred_element_type=jnp.float32)
-                att_ref[:, cut] = total.astype(jnp.bfloat16)
+
+        @pl.when((v >= first) & (v < first + 4))
+        def _():
+            cut = pl.ds(pl.multiple_of((v - first) * wide, wide), wide)
+            total = jnp.dot(hall[0], wall[0, :, cut], preferred_element_type=jnp.float32)
+            for s in range(1, X):
+                total += jnp.dot(hall[s], wall[s, :, cut], preferred_element_type=jnp.float32)
+            att_ref[:, cut] = total.astype(jnp.bfloat16)
 
         return carry
 
@@ -516,7 +543,7 @@
             pltpu.VMEM((D, FF), bf16),
             pltpu.VMEM((FF, D), bf16),
             pltpu.VMEM((X, cols, D), bf16),
-            pltpu.VMEM((2, rows + WINDOW, 2 * HEAD_DIM), bf16),
+            pltpu.VMEM((2, 2 * HEAD_DIM, rows + WINDOW), bf16),
             pltpu.VMEM((X, rows // X, cols), bf16),
             pltpu.VMEM((X, rows // X, cols), bf16),
             dma((4,)),
@@ -543,11 +570,11 @@
     )(
         moe_input,
         norm_gain.reshape(1, D),
-        routes,
-        route_weight,
+        routes.T,
+        route_weight.T,
         queries,
-        head_keys,
-        head_values,
+        head_keys.T,
+        head_values.T,
         sink_logits,
         out_weight,
         gate_weight,

time: 135 us -> 114 us (0.84)
  Pallas kernels: 125 us -> 110 us
  local copies, waits for them, and re-layouts: 9.45 us -> 3.16 us
    pallas_call x1, Pallas kernels: 125 us -> 110 us  [on_device(): pl.pallas_call(functools.partial(kernel, Z, L, X, S), out_shape=(jax.Shap...]
    unnamed x8 -> x4, local copies, waits for them, and re-layouts: 9.45 us -> 3.16 us
where the time goes in v2:
time: 114 us
  Pallas kernels  110 us (96%)
  local copies, waits for them, and re-layouts  3.16 us (3%)
    pallas_call x1, Pallas kernels, on_device(): pl.pallas_call(functools.partial(kernel, Z, L, X, S), out_shape=(jax.Shap...  110 us
    unnamed x4, local copies, waits for them, and re-layouts  3.16 us

profile of v2, /device:TPU:1, one launch (start us, length us, event | category | flops | bytes accessed | tf_op | source)
XLA Modules:
  0.0 113.7 jit_solution(16164688908101125857)
XLA Ops:
  0.6 109.9 %shard_map.131 = (bf16[256,2048]{1,0:T(8,128)(2,1)}, bf16[128,2048]{1,0:T(8,128)(2,1)}) custom-call(bf16[128,2048]{1,0:T(8,128)(2,1)} %x_ref.1, f32[1,2048]{1,0:T(1,128)} %bitcast.7, s32[4,128]{1,0:T(4,128)} %bitcast.8, f32[4,128]{1,0:T(4,128)} %bitcast.9, bf16[1024,256]{1,0:T(8,128)(2,1)} %q_ref.1, bf16[64,1024]{1,0:T(8,128)(2,1)} %bitcast.5, ...), custom_call_target="tpu_custom_call" | custom-call | tf_op jit(solution)/shard_map/pallas_call | solution.py:523
  110.6 0.0 copy-start
  110.6 2.4 %copy.16 = bf16[256,2048]{1,0:T(8,128)(2,1)} copy(bf16[256,2048]{1,0:T(8,128)(2,1)} %get-tuple-element.4) | data formatting | bytes 2097152
  112.9 0.0 copy-done
  112.9 0.8 copy.17
Async XLA Ops:
  110.6 2.4 %copy-start = (bf16[128,2048]{1,0:T(8,128)(2,1)S(1)}, bf16[128,2048]{1,0:T(8,128)(2,1)}, u32[]{:S(2)}) copy-start(bf16[128,2048]{1,0:T(8,128)(2,1)} %get-tuple-element.5) | copy-start | bytes 1572868

commit v3 on v2

--- a/solution.py
+++ b/solution.py
@@ -13,10 +13,9 @@
 CAP = 16
 EPSILON = 1e-05
 NEGATIVE = -1e30
-PIECES = 4
-AHEAD = 4
-EARLY = 3
-FILL = 1
+PIECES = 8
+AHEAD = 6
+LATE = 2
 
 
 def clamped_unit(gate_pre, up_pre):
@@ -36,6 +35,20 @@
     L,
     X,
     S,
+    x_hbm,
+    gain_hbm,
+    routes_hbm,
+    rweight_hbm,
+    q_hbm,
+    k_hbm,
+    v_hbm,
+    sink_hbm,
+    ow_hbm,
+    gw_hbm,
+    uw_hbm,
+    dw_hbm,
+    att_ref,
+    out_ref,
     x_ref,
     gain_ref,
     routes_ref,
@@ -44,12 +57,6 @@
     k_ref,
     v_ref,
     sink_ref,
-    ow_hbm,
-    gw_hbm,
-    uw_hbm,
-    dw_hbm,
-    att_ref,
-    out_ref,
     ag,
     tab,
     pick,
@@ -109,12 +116,21 @@
     right_ep = (lax.rem(ep + 1, EP), x)
     left_ep = (lax.rem(ep + EP - 1, EP), x)
 
-    loads = [
-        pltpu.make_async_copy(ow_hbm, wall.at[x], ld_sem.at[0]),
-        pltpu.make_async_copy(gw_hbm.at[0], gw, ld_sem.at[1]),
-        pltpu.make_async_copy(uw_hbm.at[0], uw, ld_sem.at[2]),
-        pltpu.make_async_copy(dw_hbm.at[0], dw, ld_sem.at[3]),
+    pairs = [
+        (x_hbm, x_ref),
+        (gain_hbm, gain_ref),
+        (routes_hbm, routes_ref),
+        (rweight_hbm, rweight_ref),
+        (k_hbm, k_ref),
+        (v_hbm, v_ref),
+        (ow_hbm, wall.at[x]),
+        (q_hbm, q_ref),
+        (sink_hbm, sink_ref),
+        (gw_hbm.at[0], gw),
+        (uw_hbm.at[0], uw),
+        (dw_hbm.at[0], dw),
     ]
+    loads = [pltpu.make_async_copy(a, b, ld_sem.at[n]) for n, (a, b) in enumerate(pairs)]
     barrier = pltpu.get_barrier_semaphore()
     met = [dev_z(1), dev_z(-1)]
     met += [dev_l(lax.rem(me + r, L)) for r in range(1, L)]
@@ -122,14 +138,20 @@
     met += [right_ep, left_ep]
     for target in met:
         pl.semaphore_signal(barrier, inc=1, device_id=target, device_id_type=MESH)
-    for load in loads:
+    for load in loads[:6]:
         load.start()
 
+    for load in loads[:2]:
+        load.wait()
     values32 = x_ref[...].astype(jnp.float32)
     scale = lax.rsqrt(jnp.mean(values32 * values32, axis=-1, keepdims=True) + EPSILON)
     normed = (values32 * scale * gain_ref[...]).astype(jnp.bfloat16)
     for f in range(S):
         ag[0, f] = normed[:, f * DS : (f + 1) * DS]
+    for load in loads[2:6]:
+        load.wait()
+    for load in loads[6:]:
+        load.start()
     tab[0, 0:4] = routes_ref[...].astype(jnp.float32)
     tab[0, 4:8] = rweight_ref[...]
     for half in range(2):
@@ -270,10 +292,10 @@
         return odd * (Z - h) + (1 - odd) * h
 
     make_slots(0)
-    for f in range(EARLY):
+    for f in range(S):
         dispatch(0, f)
 
-    loads[0].wait()
+    loads[6].wait()
 
     def weight_copy(r):
         return pltpu.make_async_remote_copy(
@@ -287,6 +309,9 @@
 
     for r in range(1, X):
         weight_copy(r).start()
+
+    for load in loads[7:9]:
+        load.wait()
 
     blocks = rows // WINDOW
 
@@ -344,7 +369,7 @@
             device_id_type=MESH,
         ).start()
 
-    for load in loads[1:]:
+    for load in loads[9:]:
         load.wait()
 
     def spread_step(u, carry):
@@ -372,12 +397,16 @@
 
             make_slots(Z - hop)
 
-        dispatch(Z - hop, i)
-        dispatch(hop, S - 1 - i)
+
+        @pl.when((u < S - LATE) | (u >= S))
+        def _():
+            dispatch(Z - hop, i)
+            dispatch(hop, S - 1 - i)
+
         half = S // 2
         k = u // half - 2
 
-        @pl.when((lax.rem(u, half) == 0) & (k >= 1))
+        @pl.when((lax.rem(u, half) == 0) & (k >= 3))
         def _():
             expert(job_offset(k))
 
@@ -394,16 +423,19 @@
         give_back(Z - hop, i)
         give_back(hop, S - 1 - i)
 
-    first_late = max(1, Z - 3)
+    first_late = max(3, Z - 3)
 
     def late_job(k, carry):
         expert(job_offset(k))
+
+        @pl.when(k == Z - 2)
+        def _():
+            for u in range(S - LATE, S):
+                dispatch(Z - 1, u)
+                dispatch(1, S - 1 - u)
+
         return carry
 
-    for f in range(EARLY, S):
-        dispatch(0, f)
-    for u in range(FILL):
-        back_unit(u)
     lax.fori_loop(first_late, Z, late_job, 0)
 
     ahead = min(AHEAD, U)
@@ -428,15 +460,19 @@
         u = U - 1 - v
         hop, i = u // S + 1, lax.rem(u, S)
 
-        @pl.when(u - ahead >= FILL)
+        @pl.when(u >= ahead)
         def _():
             back_unit(u - ahead)
 
-        @pl.when(v == 1)
+        @pl.when(v == U - 1 - S - ahead)
         def _():
             expert(0)
 
-        @pl.when(u == ahead + FILL - 1)
+        @pl.when((v >= U - 3 - S - ahead) & (v < U - 1 - S - ahead))
+        def _():
+            expert(lax.rem((v - (U - 3 - S - ahead)) * 2 + Z - 1, Z))
+
+        @pl.when(u == ahead - 1)
         def _():
             for f in range(S):
                 give_back(0, f)
@@ -478,7 +514,8 @@
         rs_copy(0, S - 1 - f).wait_recv()
         rs_copy(1, f).wait_recv()
         value = value + rs_in[0, S - 1 - f].astype(jnp.float32) + rs_in[1, f].astype(jnp.float32)
-        out_ref[:, f * DS : (f + 1) * DS] = value.astype(jnp.bfloat16)
+        cut = slice(f * DS, (f + 1) * DS)
+        out_ref[:, cut] = value.astype(jnp.bfloat16)
 
     bytes_wait(tab.at[pl.ds(0, Z - 1)], tab_send)
     for direction in range(2):
@@ -517,18 +554,25 @@
     U = (H - 1) * S + S // 2
     slots = L * CAP
     bf16, f32 = jnp.bfloat16, jnp.float32
-    vmem = pl.BlockSpec(memory_space=pltpu.VMEM)
     hbm = pl.BlockSpec(memory_space=pl.ANY)
     dma = pltpu.SemaphoreType.DMA
     attention_out, routed_out = pl.pallas_call(
         functools.partial(kernel, Z, L, X, S),
         out_shape=(
-            jax.ShapeDtypeStruct((rows // X, D), bf16),
-            jax.ShapeDtypeStruct((T, D), bf16),
+            pltpu.VMEM((rows // X, D), bf16),
+            pltpu.VMEM((T, D), bf16),
         ),
-        in_specs=[vmem] * 7 + [pl.BlockSpec(memory_space=pltpu.SMEM)] + [hbm] * 4,
-        out_specs=(vmem, vmem),
+        in_specs=[hbm] * 12,
+        out_specs=(pl.BlockSpec(memory_space=pltpu.VMEM),) * 2,
         scratch_shapes=[
+            pltpu.VMEM((T, D), bf16),
+            pltpu.VMEM((1, D), f32),
+            pltpu.VMEM(routes.shape[::-1], jnp.int32),
+            pltpu.VMEM(routes.shape[::-1], f32),
+            pltpu.VMEM((rows, cols), bf16),
+            pltpu.VMEM((HEAD_DIM, rows), bf16),
+            pltpu.VMEM((HEAD_DIM, rows), bf16),
+            pltpu.SMEM(sink_logits.shape, f32),
             pltpu.VMEM((Z, S, T, DS), bf16),
             pltpu.VMEM((Z, 8, T), f32),
             pltpu.VMEM((Z, slots, T), bf16),
@@ -546,7 +590,7 @@
             pltpu.VMEM((2, 2 * HEAD_DIM, rows + WINDOW), bf16),
             pltpu.VMEM((X, rows // X, cols), bf16),
             pltpu.VMEM((X, rows // X, cols), bf16),
-            dma((4,)),
+            dma((12,)),
             dma,
             dma((Z,)),
             dma((2,)),
@@ -581,7 +625,24 @@
         up_weight,
         down_weight,
     )
-    return (attention_out, routed_out)
+    return write_out(attention_out, routed_out)
+
+
+def write_out(*arrays):
+    def body(*refs):
+        copies = [pltpu.make_async_copy(refs[n], refs[2 + n], refs[4].at[n]) for n in range(2)]
+        for copy in copies:
+            copy.start()
+        for copy in copies:
+            copy.wait()
+
+    return pl.pallas_call(
+        body,
+        out_shape=tuple(jax.ShapeDtypeStruct(a.shape, a.dtype) for a in arrays),
+        in_specs=[pl.BlockSpec(memory_space=pltpu.VMEM)] * 2,
+        out_specs=(pl.BlockSpec(memory_space=pl.ANY),) * 2,
+        scratch_shapes=[pltpu.SemaphoreType.DMA((2,))],
+    )(*[pltpu.with_memory_space_constraint(a, pltpu.VMEM) for a in arrays])
 
 
 def solution(mesh, layer=8):

time: 114 us -> 110 us (0.965)
  local copies, waits for them, and re-layouts: 3.16 us -> 0 us
    unnamed x4 -> x0, local copies, waits for them, and re-layouts: 3.16 us -> none
    pallas_call x1 -> x2, Pallas kernels: 110 us -> 109 us  [the longest x1 108 us: on_device(): pl.pallas_call(functools.partial(kernel, Z, L, X, S), out_shape=(pltpu.VM...]
where the time goes in v3:
time: 110 us
  Pallas kernels  109 us (99%)
    pallas_call x1, Pallas kernels, on_device(): pl.pallas_call(functools.partial(kernel, Z, L, X, S), out_shape=(pltpu.VM...  108 us

profile of v3, /device:TPU:1, one launch (start us, length us, event | category | flops | bytes accessed | tf_op | source)
XLA Modules:
  0.0 109.5 jit_solution(12465984849000871866)
XLA Ops:
  0.6 107.7 %shard_map.131 = (bf16[256,2048]{1,0:T(8,128)(2,1)S(1)}, bf16[128,2048]{1,0:T(8,128)(2,1)S(1)}) custom-call(bf16[128,2048]{1,0:T(8,128)(2,1)} %x_hbm.1, f32[1,2048]{1,0:T(1,128)} %bitcast.7, s32[4,128]{1,0:T(4,128)} %bitcast.8, f32[4,128]{1,0:T(4,128)} %bitcast.9, bf16[1024,256]{1,0:T(8,128)(2,1)} %q_hbm.1, bf16[64,1024]{1,0:T(8,128)(2,1)} %bitcast.5, ...), custom_call_target="tpu_custom_call" | custom-call | tf_op jit(solution)/shard_map/pallas_call | solution.py:559
  108.4 1.2 %shard_map.132 = (bf16[256,2048]{1,0:T(8,128)(2,1)}, bf16[128,2048]{1,0:T(8,128)(2,1)}) custom-call(bf16[256,2048]{1,0:T(8,128)(2,1)S(1)} %get-tuple-element.4.refs_0_, bf16[128,2048]{1,0:T(8,128)(2,1)S(1)} %get-tuple-element.5.refs_1_), custom_call_target="tpu_custom_call" | custom-call | tf_op jit(solution)/shard_map/pallas_call | solution.py:639

commit v4 on v3

--- a/solution.py
+++ b/solution.py
@@ -15,7 +15,8 @@
 NEGATIVE = -1e30
 PIECES = 8
 AHEAD = 6
-LATE = 2
+LATE = 1
+OWN = 2
 
 
 def clamped_unit(gate_pre, up_pre):
@@ -433,6 +434,9 @@
             for u in range(S - LATE, S):
                 dispatch(Z - 1, u)
                 dispatch(1, S - 1 - u)
+            expert(0)
+            for f in range(OWN):
+                give_back(0, f)
 
         return carry
 
@@ -464,17 +468,13 @@
         def _():
             back_unit(u - ahead)
 
-        @pl.when(v == U - 1 - S - ahead)
-        def _():
-            expert(0)
-
         @pl.when((v >= U - 3 - S - ahead) & (v < U - 1 - S - ahead))
         def _():
             expert(lax.rem((v - (U - 3 - S - ahead)) * 2 + Z - 1, Z))
 
         @pl.when(u == ahead - 1)
         def _():
-            for f in range(S):
+            for f in range(OWN, S):
                 give_back(0, f)
 
         for direction in range(2):

time: 110 us -> 108 us (0.982)
  Pallas kernels: 109 us -> 107 us
    pallas_call x1, Pallas kernels: 108 us -> 106 us  [on_device(): pl.pallas_call(functools.partial(kernel, Z, L, X, S), out_shape=(pltpu.VM...]
where the time goes in v4:
time: 108 us
  Pallas kernels  107 us (99%)
    pallas_call x1, Pallas kernels, on_device(): pl.pallas_call(functools.partial(kernel, Z, L, X, S), out_shape=(pltpu.VM...  106 us

profile of v4, /device:TPU:1, one launch (start us, length us, event | category | flops | bytes accessed | tf_op | source)
XLA Modules:
  0.0 108.1 jit_solution(15782063488837543996)
XLA Ops:
  0.6 106.3 %shard_map.131 = (bf16[256,2048]{1,0:T(8,128)(2,1)S(1)}, bf16[128,2048]{1,0:T(8,128)(2,1)S(1)}) custom-call(bf16[128,2048]{1,0:T(8,128)(2,1)} %x_hbm.1, f32[1,2048]{1,0:T(1,128)} %bitcast.7, s32[4,128]{1,0:T(4,128)} %bitcast.8, f32[4,128]{1,0:T(4,128)} %bitcast.9, bf16[1024,256]{1,0:T(8,128)(2,1)} %q_hbm.1, bf16[64,1024]{1,0:T(8,128)(2,1)} %bitcast.5, ...), custom_call_target="tpu_custom_call" | custom-call | tf_op jit(solution)/shard_map/pallas_call | solution.py:559
  107.0 1.2 %shard_map.132 = (bf16[256,2048]{1,0:T(8,128)(2,1)}, bf16[128,2048]{1,0:T(8,128)(2,1)}) custom-call(bf16[256,2048]{1,0:T(8,128)(2,1)S(1)} %get-tuple-element.4.refs_0_, bf16[128,2048]{1,0:T(8,128)(2,1)S(1)} %get-tuple-element.5.refs_1_), custom_call_target="tpu_custom_call" | custom-call | tf_op jit(solution)/shard_map/pallas_call | solution.py:639

commit v5 on v4

--- a/solution.py
+++ b/solution.py
@@ -149,46 +149,7 @@
     normed = (values32 * scale * gain_ref[...]).astype(jnp.bfloat16)
     for f in range(S):
         ag[0, f] = normed[:, f * DS : (f + 1) * DS]
-    for load in loads[2:6]:
-        load.wait()
-    for load in loads[6:]:
-        load.start()
-    tab[0, 0:4] = routes_ref[...].astype(jnp.float32)
-    tab[0, 4:8] = rweight_ref[...]
-    for half in range(2):
-        cut = slice(half * HEAD_DIM, (half + 1) * HEAD_DIM)
-        kv2[0, cut, WINDOW:] = k_ref[...]
-        kv2[1, cut, WINDOW:] = v_ref[...]
-
     pl.semaphore_wait(barrier, len(met))
-
-    halo = pltpu.make_async_remote_copy(
-        src_ref=kv2.at[:, :, pl.ds(rows, WINDOW)],
-        dst_ref=kv2.at[:, :, pl.ds(0, WINDOW)],
-        send_sem=halo_send,
-        recv_sem=halo_recv,
-        device_id=right_ep,
-        device_id_type=MESH,
-    )
-    halo.start()
-
-    def tab_copy(direction, hop):
-        if direction == 0:
-            src, dst, target = lax.rem(Z - hop + 1, Z), Z - hop, dev_z(1)
-        else:
-            src, dst, target = hop - 1, hop, dev_z(-1)
-        return pltpu.make_async_remote_copy(
-            src_ref=tab.at[src],
-            dst_ref=tab.at[dst],
-            send_sem=tab_send,
-            recv_sem=tab_recv.at[dst],
-            device_id=target,
-            device_id_type=MESH,
-        )
-
-    tab_copy(0, 1).start()
-    if H > 1:
-        tab_copy(1, 1).start()
 
     def ring_copy(direction, u):
         hop, i = u // S + 1, lax.rem(u, S)
@@ -205,7 +166,50 @@
             device_id_type=MESH,
         )
 
-    for u in range(min(S, U)):
+    for u in range(2):
+        ring_copy(0, u).start()
+        ring_copy(1, u).start()
+
+    for load in loads[2:6]:
+        load.wait()
+    for load in loads[6:]:
+        load.start()
+    tab[0, 0:4] = routes_ref[...].astype(jnp.float32)
+    tab[0, 4:8] = rweight_ref[...]
+    for half in range(2):
+        cut = slice(half * HEAD_DIM, (half + 1) * HEAD_DIM)
+        kv2[0, cut, WINDOW:] = k_ref[...]
+        kv2[1, cut, WINDOW:] = v_ref[...]
+
+    halo = pltpu.make_async_remote_copy(
+        src_ref=kv2.at[:, :, pl.ds(rows, WINDOW)],
+        dst_ref=kv2.at[:, :, pl.ds(0, WINDOW)],
+        send_sem=halo_send,
+        recv_sem=halo_recv,
+        device_id=right_ep,
+        device_id_type=MESH,
+    )
+    halo.start()
+
+    def tab_copy(direction, hop):
+        if direction == 0:
+            src, dst, target = lax.rem(Z - hop + 1, Z), Z - hop, dev_z(1)
+        else:
+            src, dst, target = hop - 1, hop, dev_z(-1)
+        return pltpu.make_async_remote_copy(
+            src_ref=tab.at[src],
+            dst_ref=tab.at[dst],
+            send_sem=tab_send,
+            recv_sem=tab_recv.at[dst],
+            device_id=target,
+            device_id_type=MESH,
+        )
+
+    tab_copy(0, 1).start()
+    if H > 1:
+        tab_copy(1, 1).start()
+
+    for u in range(2, S):
         ring_copy(0, u).start()
         ring_copy(1, u).start()
 
@@ -477,7 +481,7 @@
             for f in range(OWN, S):
                 give_back(0, f)
 
-        for direction in range(2):
+        for direction in (1, 0):
             o, f = (hop, S - 1 - i) if direction == 0 else (Z - hop, i)
             value = combine(o, f)
 

time: 108 us -> 108 us (level)
  no operation moved by 1% of the time
where the time goes in v5:
time: 108 us
  Pallas kernels  107 us (99%)
    pallas_call x1, Pallas kernels, on_device(): pl.pallas_call(functools.partial(kernel, Z, L, X, S), out_shape=(pltpu.VM...  106 us

profile of v5, /device:TPU:1, one launch (start us, length us, event | category | flops | bytes accessed | tf_op | source)
XLA Modules:
  0.0 108.1 jit_solution(2990825242380731412)
XLA Ops:
  0.6 106.3 %shard_map.131 = (bf16[256,2048]{1,0:T(8,128)(2,1)S(1)}, bf16[128,2048]{1,0:T(8,128)(2,1)S(1)}) custom-call(bf16[128,2048]{1,0:T(8,128)(2,1)} %x_hbm.1, f32[1,2048]{1,0:T(1,128)} %bitcast.7, s32[4,128]{1,0:T(4,128)} %bitcast.8, f32[4,128]{1,0:T(4,128)} %bitcast.9, bf16[1024,256]{1,0:T(8,128)(2,1)} %q_hbm.1, bf16[64,1024]{1,0:T(8,128)(2,1)} %bitcast.5, ...), custom_call_target="tpu_custom_call" | custom-call | tf_op jit(solution)/shard_map/pallas_call | solution.py:563
  107.0 1.2 %shard_map.132 = (bf16[256,2048]{1,0:T(8,128)(2,1)}, bf16[128,2048]{1,0:T(8,128)(2,1)}) custom-call(bf16[256,2048]{1,0:T(8,128)(2,1)S(1)} %get-tuple-element.4.refs_0_, bf16[128,2048]{1,0:T(8,128)(2,1)S(1)} %get-tuple-element.5.refs_1_), custom_call_target="tpu_custom_call" | custom-call | tf_op jit(solution)/shard_map/pallas_call | solution.py:643
